TPU v7x, 128 devices: a whole 4x4x4 slice. The times are simulated.
128 devices in a mesh: ra: 16 (over z, x), cb: 8 (over y, core).
Axes of the slice: x: 4, y: 4, z: 4, core: 2. Of those that a mesh axis runs over, the one named last changes fastest.
Arguments:
- inputs: bfloat16 [1536, 4096], P(None, 'ra'), may hold values from -12 to 12
- gate_weight: bfloat16 [2, 4096, 11264], P(None, 'ra', 'cb'), may hold values from -0.09375 to 0.09375
- up_weight: bfloat16 [2, 4096, 11264], P(None, 'ra', 'cb'), may hold values from -0.09375 to 0.09375
- down_weight: bfloat16 [2, 11264, 4096], P(None, 'cb', 'ra'), may hold values from -0.0546875 to 0.0546875
- norm_gain: float32 [2, 4096], P(None, 'ra'), may hold values from 0.05 to 8
- norm_shift: float32 [2, 4096], P(None, 'ra'), may hold values from -1.5 to 1.5
Outputs:
- outputs: bfloat16 [1536, 4096], P(None, 'ra')
All inputs are finite; a program needn't handle non-finite values.
Results may differ from a plain program's by a relative error of at most 0.04.
Values may be sent and summed in bfloat16 or wider, within the bound.
No kernel may reach another device: no remote copies, remote signals or barrier semaphores. Data moves between devices by JAX's collectives and lax.ppermute only.
A program may use at most 64 MiB of HBM per device.

v0:
```python
import jax
import jax.numpy as jnp
from jax import lax
from jax.sharding import Mesh
from jax.sharding import PartitionSpec as P

RESIDUAL = 0.5
EPSILON = 1e-05
BF16 = jnp.bfloat16
F32 = jnp.float32


def exchange(parts, axes):
    return lax.all_to_all(parts, axes, 0, 0, tiled=True)


def share(block, axes, peers):
    return exchange(jnp.broadcast_to(block[None], (peers, *block.shape)), axes)


def swap_core(block):
    return lax.ppermute(block, "c", [(0, 1), (1, 0)])


def dot_nt(a, b):
    return lax.dot_general(a, b, (((1,), (1,)), ((), ())), preferred_element_type=F32)


def regroup_weights(gate, up, down):
    stacked = jnp.stack((gate.T, up.T, down))
    rows = stacked.shape[1] // 4
    parts = stacked.reshape(3, 4, rows, 256).transpose(1, 0, 2, 3)
    mine = exchange(parts, "x")
    mine = mine.transpose(1, 2, 0, 3).reshape(3, rows, 1024)
    other = swap_core(mine)
    both = jnp.concatenate((mine, other), axis=1)
    return (both[:2].reshape(2 * 2 * rows, 1024), both[2])


def normed(mixed, row_sum, row_squares, gain, shift):
    mean = row_sum / 4096.0
    var = row_squares / 4096.0 - mean * mean
    out = (mixed - mean[:, None]) * lax.rsqrt(var + EPSILON)[:, None]
    return (out * gain + shift).astype(BF16)


def hidden_units(stream, w_gu):
    partial = dot_nt(stream, w_gu).astype(BF16)
    cols = partial.shape[1] // 2
    summed = exchange(partial.reshape(4, -1, 2 * cols), "z").astype(F32).sum(axis=0)
    hidden = (jax.nn.silu(summed[:, :cols]) * summed[:, cols:]).astype(BF16)
    return share(hidden, "z", 4).reshape(-1, cols)


def per_device(inputs, gate_weight, up_weight, down_weight, norm_gain, norm_shift):
    c = lax.axis_index("c")
    x = lax.axis_index("x")
    y = lax.axis_index("y")
    half = inputs.shape[0] // 2
    quarter = half // 4
    mine = lax.dynamic_slice_in_dim(inputs, c * half + y * quarter, quarter, 0)
    rows = share(mine, "x", 4).transpose(1, 0, 2).reshape(quarter, 1024)
    stream = share(rows, "y", 4).reshape(half, 1024)
    affine = jnp.stack((norm_gain[0], norm_shift[0]))
    affine = lax.all_gather(affine, "x", axis=1, tiled=True)
    gu0, down0 = regroup_weights(gate_weight[0], up_weight[0], down_weight[0])
    gu1, down1 = regroup_weights(gate_weight[1], up_weight[1], down_weight[1])
    hidden = hidden_units(stream, gu0)
    partial = jnp.dot(hidden, down0, preferred_element_type=F32).astype(BF16)
    block = half // 16
    branch = exchange(partial.reshape(16, block, 1024), ("x", "y")).astype(F32).sum(axis=0)
    own = lax.dynamic_slice_in_dim(stream, (x * 4 + y) * block, block, 0)
    mixed = RESIDUAL * own.astype(F32) + branch
    stats = lax.psum(jnp.stack((mixed.sum(axis=1), (mixed * mixed).sum(axis=1))), "z")
    out = normed(mixed, stats[0], stats[1], affine[0], affine[1])
    stream = share(out, ("x", "y"), 16).reshape(half, 1024)
    hidden = hidden_units(stream, gu1)
    partial = jnp.dot(hidden, down1, preferred_element_type=F32).astype(BF16)
    parts = partial.reshape(4, quarter, 4, 256).transpose(2, 0, 1, 3).reshape(16, quarter, 256)
    branch = exchange(parts, ("x", "y")).astype(F32).sum(axis=0)
    own = lax.dynamic_slice(stream, (y * quarter, x * 256), (quarter, 256))
    mixed = RESIDUAL * own.astype(F32) + branch
    stats = lax.psum(jnp.stack((mixed.sum(axis=1), (mixed * mixed).sum(axis=1))), ("z", "x"))
    out = normed(mixed, stats[0], stats[1], norm_gain[1], norm_shift[1])
    ours = share(out, "y", 4).reshape(half, 256)
    theirs = swap_core(ours)
    result = jnp.concatenate((ours, theirs), axis=0)
    swapped = jnp.concatenate((theirs, ours), axis=0)
    return jnp.where(c == 0, result, swapped)


def solution(mesh):
    finer = Mesh(mesh.devices.reshape(4, 4, 4, 2), ("z", "x", "y", "c"))
    ra, cb = (("z", "x"), ("y", "c"))
    in_specs = (
        P(None, ra),
        P(None, ra, cb),
        P(None, ra, cb),
        P(None, cb, ra),
        P(None, ra),
        P(None, ra),
    )
    return jax.shard_map(
        per_device, mesh=finer, in_specs=in_specs, out_specs=P(None, ra), check_vma=False
    )
```

profile of v0, /device:TPU:1, one launch (start us, length us, event | category | flops | bytes accessed | tf_op | source)
XLA Modules:
  0.0 365.9 jit_solution(2115882943331297913)
XLA Ops:
  7.9 30.5 %all_to_all.60 = bf16[4,3,352,256]{3,2,1,0:T(8,128)(2,1)S(1)} all-to-all(bf16[4,3,352,256]{3,2,1,0:T(8,128)(2,1)S(1)} %copy.30), channel_id=1, replica_groups=mesh['z'=4,'x'=4,'y'=4,'c'=2] {'x'}, dimensions={0} | all-to-all | bytes 4325376 | tf_op jit(solution)/shard_map/all_to_all | solution.py:14
  41.0 10.2 %all_to_all.61 = bf16[4,192,256]{2,1,0:T(8,128)(2,1)S(1)} all-to-all(bf16[4,192,256]{2,1,0:T(8,128)(2,1)S(1)} %broadcast_in_dim.14), channel_id=1, replica_groups=mesh['z'=4,'x'=4,'y'=4,'c'=2] {'x'}, dimensions={0} | all-to-all | bytes 786432 | tf_op jit(solution)/shard_map/all_to_all | solution.py:14
  52.7 4.4 %all-to-all-start.1 = ((bf16[4,192,1024]{2,1,0:T(8,128)(2,1)}), bf16[4,192,1024]{2,1,0:T(8,128)(2,1)}, u32[]{:S(2)}, u32[]{:S(2)}) async-start(bf16[4,192,1024]{2,1,0:T(8,128)(2,1)} %broadcast_in_dim.16), calls=%async_computation.1 | async-start | bytes 3145728 | tf_op jit(solution)/shard_map/all_to_all | solution.py:14
  62.9 13.6 %all-to-all-done.1 = bf16[4,192,1024]{2,1,0:T(8,128)(2,1)} async-done(((bf16[4,192,1024]{2,1,0:T(8,128)(2,1)}), bf16[4,192,1024]{2,1,0:T(8,128)(2,1)}, u32[]{:S(2)}, u32[]{:S(2)}) %all-to-all-start.1) | async-done | bytes 1572896 | tf_op jit(solution)/shard_map/all_to_all | solution.py:14
  76.5 4.9 %convolution_convert_fusion.1 = bf16[768,1408]{1,0:T(8,128)(2,1)S(1)} fusion(bf16[768,1024]{1,0:T(8,128)(2,1)} %bitcast.1, bf16[1408,1024]{1,0:T(8,128)(2,1)} %bitcast.85), kind=kOutput, calls=%fused_computation.3 | convolution fusion | flops 2215673856 | bytes 6619136 | tf_op jit(solution)/shard_map/dot_general | solution.py:26
  81.5 29.2 %all_to_all.62 = bf16[4,192,1408]{2,1,0:T(8,128)(2,1)S(1)} all-to-all(bf16[4,192,1408]{2,1,0:T(8,128)(2,1)S(1)} %bitcast.93), channel_id=1, replica_groups=mesh['z'=4,'x'=4,'y'=4,'c'=2] {'z'}, dimensions={0} | all-to-all | bytes 4325376 | tf_op jit(solution)/shard_map/all_to_all | solution.py:14
  112.4 4.4 %all-to-all-start.4 = ((bf16[4,192,704]{2,1,0:T(8,128)(2,1)}), bf16[4,192,704]{2,1,0:T(8,128)(2,1)}, u32[]{:S(2)}, u32[]{:S(2)}) async-start(bf16[4,192,704]{2,1,0:T(8,128)(2,1)} %broadcast_in_dim.17), calls=%async_computation.4 | async-start | bytes 2359296 | tf_op jit(solution)/shard_map/all_to_all | solution.py:14
  119.1 10.4 %all-to-all-done.4 = bf16[4,192,704]{2,1,0:T(8,128)(2,1)} async-done(((bf16[4,192,704]{2,1,0:T(8,128)(2,1)}), bf16[4,192,704]{2,1,0:T(8,128)(2,1)}, u32[]{:S(2)}, u32[]{:S(2)}) %all-to-all-start.4) | async-done | bytes 1081376 | tf_op jit(solution)/shard_map/all_to_all | solution.py:14
  133.2 4.3 %convolution_convert_fusion.3 = bf16[768,1024]{1,0:T(8,128)(2,1)} fusion(bf16[768,704]{1,0:T(8,128)(2,1)} %bitcast.13, bf16[3,704,1024]{2,1,0:T(8,128)(2,1)} %copy-done.2), kind=kOutput, calls=%fused_computation.9 | convolution fusion | flops 1108082688 | bytes 4194304 | tf_op jit(solution)/shard_map/dot_general | solution.py:69
  137.5 18.0 %all-to-all-done.7 = bf16[4,3,352,256]{3,2,1,0:T(8,128)(2,1)S(1)} async-done(((bf16[4,3,352,256]{3,2,1,0:T(8,128)(2,1)}), bf16[4,3,352,256]{3,2,1,0:T(8,128)(2,1)S(1)}, u32[]{:S(2)}, u32[]{:S(2)}) %all-to-all-start.7) | async-done | bytes 2162720 | tf_op jit(solution)/shard_map/all_to_all | solution.py:14
  155.5 4.4 %all-to-all-start.5 = ((bf16[16,48,1024]{2,1,0:T(8,128)(2,1)}), bf16[16,48,1024]{2,1,0:T(8,128)(2,1)}, u32[]{:S(2)}, u32[]{:S(2)}) async-start(bf16[16,48,1024]{2,1,0:T(8,128)(2,1)} %bitcast.95), calls=%async_computation.5 | async-start | bytes 3145728 | tf_op jit(solution)/shard_map/all_to_all | solution.py:14
  160.0 18.8 %all_gather.3 = f32[2,1024]{1,0:T(2,128)S(1)} all-gather(f32[2,256]{1,0:T(2,128)S(1)} %pad_maximum_fusion), channel_id=1, replica_groups=mesh['z'=4,'x'=4,'y'=4,'c'=2] {'x'}, dimensions={1}, use_global_device_ids=true | all-gather | bytes 10240 | tf_op jit(solution)/shard_map/all_gather | solution.py:65
  180.4 8.3 %collective-permute-start.1 = (bf16[3,352,1024]{2,1,0:T(8,128)(2,1)}, bf16[3,352,1024]{2,1,0:T(8,128)(2,1)S(1)}, u32[]{:S(2)}, u32[]{:S(2)}) collective-permute-start(bf16[3,352,1024]{2,1,0:T(8,128)(2,1)} %bitcast.59), channel_id=1, source_target_pairs={{0,1},{1,0},{2,3},{3,2},{4,5},{5,4},{6,7},{7,6},{8,9},{9,8},{10,11... | collective-permute-start | bytes 6488072 | tf_op jit(solution)/shard_map/ppermute | solution.py:22
  191.5 6.9 %psum.14 = f32[2,48]{1,0:T(2,128)S(1)} all-reduce(f32[2,48]{1,0:T(2,128)S(1)} %pad_maximum_fusion.2), channel_id=1, replica_groups=mesh['z'=4,'x'=4,'y'=4,'c'=2] {'z'}, use_global_device_ids=true, to_apply=%region_4.5 | all-reduce | flops 96 | bytes 768 | tf_op jit(solution)/shard_map/psum | solution.py:74
  200.8 5.1 %all-to-all-start.6 = ((bf16[16,48,1024]{2,1,0:T(8,128)(2,1)}), bf16[16,48,1024]{2,1,0:T(8,128)(2,1)}, u32[]{:S(2)}, u32[]{:S(2)}) async-start(bf16[16,48,1024]{2,1,0:T(8,128)(2,1)} %broadcast_in_dim.18), calls=%async_computation.6 | async-start | bytes 3145728 | tf_op jit(solution)/shard_map/all_to_all | solution.py:14
  211.8 14.5 %all-to-all-done.6 = bf16[16,48,1024]{2,1,0:T(8,128)(2,1)} async-done(((bf16[16,48,1024]{2,1,0:T(8,128)(2,1)}), bf16[16,48,1024]{2,1,0:T(8,128)(2,1)}, u32[]{:S(2)}, u32[]{:S(2)}) %all-to-all-start.6) | async-done | bytes 1572896 | tf_op jit(solution)/shard_map/all_to_all | solution.py:14
  226.3 4.9 %convolution_convert_fusion = bf16[768,1408]{1,0:T(8,128)(2,1)S(1)} fusion(bf16[768,1024]{1,0:T(8,128)(2,1)} %bitcast.22, bf16[1408,1024]{1,0:T(8,128)(2,1)} %bitcast.86), kind=kOutput, calls=%fused_computation.2 | convolution fusion | flops 2215673856 | bytes 6619136 | tf_op jit(solution)/shard_map/dot_general | solution.py:26
  231.3 25.4 %all_to_all.63 = bf16[4,192,1408]{2,1,0:T(8,128)(2,1)S(1)} all-to-all(bf16[4,192,1408]{2,1,0:T(8,128)(2,1)S(1)} %bitcast.94), channel_id=1, replica_groups=mesh['z'=4,'x'=4,'y'=4,'c'=2] {'z'}, dimensions={0} | all-to-all | bytes 4325376 | tf_op jit(solution)/shard_map/all_to_all | solution.py:14
  257.4 13.7 %all_to_all.64 = bf16[4,192,704]{2,1,0:T(8,128)(2,1)S(1)} all-to-all(bf16[4,192,704]{2,1,0:T(8,128)(2,1)S(1)} %broadcast_in_dim.19), channel_id=1, replica_groups=mesh['z'=4,'x'=4,'y'=4,'c'=2] {'z'}, dimensions={0} | all-to-all | bytes 2162688 | tf_op jit(solution)/shard_map/all_to_all | solution.py:14
  279.3 10.2 %all-to-all-start.10 = ((bf16[16,192,256]{2,1,0:T(8,128)(2,1)}), bf16[16,192,256]{2,1,0:T(8,128)(2,1)S(1)}, u32[]{:S(2)}, u32[]{:S(2)}) async-start(bf16[16,192,256]{2,1,0:T(8,128)(2,1)} %bitcast.84), calls=%async_computation.10 | async-start | bytes 3145728 | tf_op jit(solution)/shard_map/all_to_all | solution.py:14
  289.6 19.0 %all-to-all-done.10 = bf16[16,192,256]{2,1,0:T(8,128)(2,1)S(1)} async-done(((bf16[16,192,256]{2,1,0:T(8,128)(2,1)}), bf16[16,192,256]{2,1,0:T(8,128)(2,1)S(1)}, u32[]{:S(2)}, u32[]{:S(2)}) %all-to-all-start.10) | async-done | bytes 1572896 | tf_op jit(solution)/shard_map/all_to_all | solution.py:14
  309.9 31.9 %psum.15 = f32[2,192]{1,0:T(2,128)S(1)} all-reduce(f32[2,192]{1,0:T(2,128)S(1)} %pad_maximum_fusion.1), channel_id=1, replica_groups=mesh['z'=4,'x'=4,'y'=4,'c'=2] {'z','x'}, use_global_device_ids=true, to_apply=%region_9.10 | all-reduce | flops 384 | bytes 3072 | tf_op jit(solution)/shard_map/psum | solution.py:83
  342.9 10.1 %all_to_all.65 = bf16[4,192,256]{2,1,0:T(8,128)(2,1)S(1)} all-to-all(bf16[4,192,256]{2,1,0:T(8,128)(2,1)S(1)} %broadcast_in_dim.20), channel_id=1, replica_groups=mesh['z'=4,'x'=4,'y'=4,'c'=2] {'y'}, dimensions={0} | all-to-all | bytes 786432 | tf_op jit(solution)/shard_map/all_to_all | solution.py:14
  353.0 10.3 %collective-permute-start.2 = (bf16[768,256]{1,0:T(8,128)(2,1)S(1)}, bf16[768,256]{1,0:T(8,128)(2,1)S(1)}, u32[]{:S(2)}, u32[]{:S(2)}) collective-permute-start(bf16[768,256]{1,0:T(8,128)(2,1)S(1)} %bitcast.97), channel_id=1, source_target_pairs={{0,1},{1,0},{2,3},{3,2},{4,5},{5,4},{6,7},{7,6},{8,9},{9,8},{10,11... | collective-permute-start | bytes 1179656 | tf_op jit(solution)/shard_map/ppermute | solution.py:22
  (74 shorter events, 51.8 us)
Async XLA Ops:
  0.0 40.9 %copy-start = (bf16[1536,256]{1,0:T(8,128)(2,1)S(1)}, bf16[1536,256]{1,0:T(8,128)(2,1)}, u32[]{:S(2)}) copy-start(bf16[1536,256]{1,0:T(8,128)(2,1)} %param.6) | copy-start | bytes 2359300
  38.7 18.5 %collective-permute-start = (bf16[3,352,1024]{2,1,0:T(8,128)(2,1)S(1)}, bf16[3,352,1024]{2,1,0:T(8,128)(2,1)}, u32[]{:S(2)}, u32[]{:S(2)}) collective-permute-start(bf16[3,352,1024]{2,1,0:T(8,128)(2,1)S(1)} %bitcast.81), channel_id=1, source_target_pairs={{0,1},{1,0},{2,3},{3,2},{4,5},{5,4},{6,7},{7,6},{8,9},{9,8},{10,11... | collective-permute-start | bytes 6488072 | tf_op jit(solution)/shard_map/ppermute | solution.py:22
  52.7 23.9 %all-to-all-start.1 = ((bf16[4,192,1024]{2,1,0:T(8,128)(2,1)}), bf16[4,192,1024]{2,1,0:T(8,128)(2,1)}, u32[]{:S(2)}, u32[]{:S(2)}) async-start(bf16[4,192,1024]{2,1,0:T(8,128)(2,1)} %broadcast_in_dim.16), calls=%async_computation.1 | async-start | bytes 3145728 | tf_op jit(solution)/shard_map/all_to_all | solution.py:14
  59.0 2.1 copy-start.2
  111.2 5.6 %copy-start.4 = (bf16[1,256,1408]{2,1,0:T(8,128)(2,1)S(1)}, bf16[1,256,1408]{2,1,0:T(8,128)(2,1)}, u32[]{:S(2)}) copy-start(bf16[1,256,1408]{2,1,0:T(8,128)(2,1)} %get-tuple-element.9) | copy-start | bytes 2162692
  112.4 4.7 %copy-start.5 = (bf16[1,256,1408]{2,1,0:T(8,128)(2,1)S(1)}, bf16[1,256,1408]{2,1,0:T(8,128)(2,1)}, u32[]{:S(2)}) copy-start(bf16[1,256,1408]{2,1,0:T(8,128)(2,1)} %get-tuple-element.11) | copy-start | bytes 2162692
  112.4 5.0 %copy-start.6 = (bf16[1,1408,256]{2,1,0:T(8,128)(2,1)S(1)}, bf16[1,1408,256]{2,1,0:T(8,128)(2,1)}, u32[]{:S(2)}) copy-start(bf16[1,1408,256]{2,1,0:T(8,128)(2,1)} %get-tuple-element.13) | copy-start | bytes 2162692
  112.4 17.1 %all-to-all-start.4 = ((bf16[4,192,704]{2,1,0:T(8,128)(2,1)}), bf16[4,192,704]{2,1,0:T(8,128)(2,1)}, u32[]{:S(2)}, u32[]{:S(2)}) async-start(bf16[4,192,704]{2,1,0:T(8,128)(2,1)} %broadcast_in_dim.17), calls=%async_computation.4 | async-start | bytes 2359296 | tf_op jit(solution)/shard_map/all_to_all | solution.py:14
  129.5 25.9 %all-to-all-start.7 = ((bf16[4,3,352,256]{3,2,1,0:T(8,128)(2,1)}), bf16[4,3,352,256]{3,2,1,0:T(8,128)(2,1)S(1)}, u32[]{:S(2)}, u32[]{:S(2)}) async-start(bf16[4,3,352,256]{3,2,1,0:T(8,128)(2,1)} %copy.34), calls=%async_computation.7 | async-start | bytes 4325376 | tf_op jit(solution)/shard_map/all_to_all | solution.py:14
  137.5 22.4 %copy-start.7 = (f32[2,256]{1,0:T(2,128)S(1)}, f32[2,256]{1,0:T(2,128)}, u32[]{:S(2)}) copy-start(f32[2,256]{1,0:T(2,128)} %param.10) | copy-start | bytes 6148
  137.5 22.5 %copy-start.8 = (f32[2,256]{1,0:T(2,128)S(1)}, f32[2,256]{1,0:T(2,128)}, u32[]{:S(2)}) copy-start(f32[2,256]{1,0:T(2,128)} %param.11) | copy-start | bytes 6148
  155.5 33.3 %all-to-all-start.5 = ((bf16[16,48,1024]{2,1,0:T(8,128)(2,1)}), bf16[16,48,1024]{2,1,0:T(8,128)(2,1)}, u32[]{:S(2)}, u32[]{:S(2)}) async-start(bf16[16,48,1024]{2,1,0:T(8,128)(2,1)} %bitcast.95), calls=%async_computation.5 | async-start | bytes 3145728 | tf_op jit(solution)/shard_map/all_to_all | solution.py:14
  180.4 27.2 %collective-permute-start.1 = (bf16[3,352,1024]{2,1,0:T(8,128)(2,1)}, bf16[3,352,1024]{2,1,0:T(8,128)(2,1)S(1)}, u32[]{:S(2)}, u32[]{:S(2)}) collective-permute-start(bf16[3,352,1024]{2,1,0:T(8,128)(2,1)} %bitcast.59), channel_id=1, source_target_pairs={{0,1},{1,0},{2,3},{3,2},{4,5},{5,4},{6,7},{7,6},{8,9},{9,8},{10,11... | collective-permute-start | bytes 6488072 | tf_op jit(solution)/shard_map/ppermute | solution.py:22
  200.8 25.5 %all-to-all-start.6 = ((bf16[16,48,1024]{2,1,0:T(8,128)(2,1)}), bf16[16,48,1024]{2,1,0:T(8,128)(2,1)}, u32[]{:S(2)}, u32[]{:S(2)}) async-start(bf16[16,48,1024]{2,1,0:T(8,128)(2,1)} %broadcast_in_dim.18), calls=%async_computation.6 | async-start | bytes 3145728 | tf_op jit(solution)/shard_map/all_to_all | solution.py:14
  207.9 2.0 copy-start.3
  279.3 29.2 %all-to-all-start.10 = ((bf16[16,192,256]{2,1,0:T(8,128)(2,1)}), bf16[16,192,256]{2,1,0:T(8,128)(2,1)S(1)}, u32[]{:S(2)}, u32[]{:S(2)}) async-start(bf16[16,192,256]{2,1,0:T(8,128)(2,1)} %bitcast.84), calls=%async_computation.10 | async-start | bytes 3145728 | tf_op jit(solution)/shard_map/all_to_all | solution.py:14
  308.6 57.3 %copy-start.1 = (bf16[1536,256]{1,0:T(8,128)(2,1)S(1)}, bf16[1536,256]{1,0:T(8,128)(2,1)}, u32[]{:S(2)}) copy-start(bf16[1536,256]{1,0:T(8,128)(2,1)} %param.6) | copy-start | bytes 2359300
  353.0 11.7 %collective-permute-start.2 = (bf16[768,256]{1,0:T(8,128)(2,1)S(1)}, bf16[768,256]{1,0:T(8,128)(2,1)S(1)}, u32[]{:S(2)}, u32[]{:S(2)}) collective-permute-start(bf16[768,256]{1,0:T(8,128)(2,1)S(1)} %bitcast.97), channel_id=1, source_target_pairs={{0,1},{1,0},{2,3},{3,2},{4,5},{5,4},{6,7},{7,6},{8,9},{9,8},{10,11... | collective-permute-start | bytes 1179656 | tf_op jit(solution)/shard_map/ppermute | solution.py:22
where the time goes:
time: 367 us; the launch traced here: 366 us
  blocking collectives  177 us (48%)
  waiting for transfers between devices  76.9 us (21%)
  starting transfers between devices  52.9 us (14%)
  local copies, waits for them, and re-layouts  31.9 us (9%)
  matrix products  18.1 us (5%)
  other arithmetic  8.87 us (2%)
    all_to_all x6, blocking collectives, exchange(): return lax.all_to_all(parts, axes, 0, 0, tiled=True)  119 us
    all_to_all x6, waiting for transfers between devices, exchange(): return lax.all_to_all(parts, axes, 0, 0, tiled=True)  75.6 us
    all_to_all x6, starting transfers between devices, exchange(): return lax.all_to_all(parts, axes, 0, 0, tiled=True)  32.1 us
    psum x1, blocking collectives, per_device(): lax.psum(jnp.stack((mixed.sum(axis=1), (mixed * mixed).sum(axis=1))), ('z...  31.9 us
    ppermute x3, starting transfers between devices, swap_core(): return lax.ppermute(block, 'c', [(0, 1), (1, 0)])  20.8 us
    all_gather x1, blocking collectives, per_device(): affine = lax.all_gather(affine, 'x', axis=1, tiled=True)  18.8 us
    dot_general x2, matrix products, dot_nt(): lax.dot_general(a, b, (((1,), (1,)), ((), ())), preferred_element_type=F32)  9.85 us
  transfers between devices with their start and end apart: 9, of which 6 were waited for; matrix products, arithmetic and copies ran while one was open for 6% of the time, Pallas kernels for 0%

commit v1 on v0

--- a/solution.py
+++ b/solution.py
@@ -80,7 +80,10 @@
     branch = exchange(parts, ("x", "y")).astype(F32).sum(axis=0)
     own = lax.dynamic_slice(stream, (y * quarter, x * 256), (quarter, 256))
     mixed = RESIDUAL * own.astype(F32) + branch
-    stats = lax.psum(jnp.stack((mixed.sum(axis=1), (mixed * mixed).sum(axis=1))), ("z", "x"))
+    stats = lax.psum(
+        lax.psum(jnp.stack((mixed.sum(axis=1), (mixed * mixed).sum(axis=1))), axis_name="z"),
+        axis_name="x",
+    )
     out = normed(mixed, stats[0], stats[1], norm_gain[1], norm_shift[1])
     ours = share(out, "y", 4).reshape(half, 256)
     theirs = swap_core(ours)

time: 367 us -> 348 us (0.948)
  blocking collectives: 177 us -> 160 us
    psum x1 -> x2, blocking collectives: 31.9 us -> 15.7 us  [the longest x1 8.82 us: per_device(): lax.psum(lax.psum(jnp.stack((mixed.sum(axis=1), (mixed * mixed).sum(axis=...]
  transfers between devices with their start and end apart: 9 -> 9, of which waited for: 6 -> 6; matrix products, arithmetic and copies ran while one was open for 6% -> 7% of each run, Pallas kernels for 0% -> 0%
where the time goes in v1:
time: 348 us; the launch traced here: 346 us
  blocking collectives  160 us (46%)
  waiting for transfers between devices  76.8 us (22%)
  starting transfers between devices  49.9 us (14%)
  local copies, waits for them, and re-layouts  31.9 us (9%)
  matrix products  18.1 us (5%)
  other arithmetic  8.87 us (3%)
    all_to_all x6, blocking collectives, exchange(): return lax.all_to_all(parts, axes, 0, 0, tiled=True)  119 us
    all_to_all x6, waiting for transfers between devices, exchange(): return lax.all_to_all(parts, axes, 0, 0, tiled=True)  75.4 us
    all_to_all x6, starting transfers between devices, exchange(): return lax.all_to_all(parts, axes, 0, 0, tiled=True)  32 us
    all_gather x1, blocking collectives, per_device(): affine = lax.all_gather(affine, 'x', axis=1, tiled=True)  18.8 us
    ppermute x3, starting transfers between devices, swap_core(): return lax.ppermute(block, 'c', [(0, 1), (1, 0)])  17.9 us
    dot_general x2, matrix products, dot_nt(): lax.dot_general(a, b, (((1,), (1,)), ((), ())), preferred_element_type=F32)  9.85 us
    psum x1, blocking collectives, per_device(): lax.psum(lax.psum(jnp.stack((mixed.sum(axis=1), (mixed * mixed).sum(axis=...  8.82 us
    unnamed x24, local copies, waits for them, and re-layouts  7.21 us
  transfers between devices with their start and end apart: 9, of which 6 were waited for; matrix products, arithmetic and copies ran while one was open for 7% of the time, Pallas kernels for 0%

profile of v1, /device:TPU:1, one launch (start us, length us, event | category | flops | bytes accessed | tf_op | source)
XLA Modules:
  0.0 346.3 jit_solution(12665493751490253051)
XLA Ops:
  7.9 30.5 %all_to_all.60 = bf16[4,3,352,256]{3,2,1,0:T(8,128)(2,1)S(1)} all-to-all(bf16[4,3,352,256]{3,2,1,0:T(8,128)(2,1)S(1)} %copy.30), channel_id=1, replica_groups=mesh['z'=4,'x'=4,'y'=4,'c'=2] {'x'}, dimensions={0} | all-to-all | bytes 4325376 | tf_op jit(solution)/shard_map/all_to_all | solution.py:14
  40.9 10.2 %all_to_all.61 = bf16[4,192,256]{2,1,0:T(8,128)(2,1)S(1)} all-to-all(bf16[4,192,256]{2,1,0:T(8,128)(2,1)S(1)} %broadcast_in_dim.14), channel_id=1, replica_groups=mesh['z'=4,'x'=4,'y'=4,'c'=2] {'x'}, dimensions={0} | all-to-all | bytes 786432 | tf_op jit(solution)/shard_map/all_to_all | solution.py:14
  52.6 4.3 %all-to-all-start.1 = ((bf16[4,192,1024]{2,1,0:T(8,128)(2,1)}), bf16[4,192,1024]{2,1,0:T(8,128)(2,1)}, u32[]{:S(2)}, u32[]{:S(2)}) async-start(bf16[4,192,1024]{2,1,0:T(8,128)(2,1)} %broadcast_in_dim.16), calls=%async_computation.1 | async-start | bytes 3145728 | tf_op jit(solution)/shard_map/all_to_all | solution.py:14
  62.9 13.6 %all-to-all-done.1 = bf16[4,192,1024]{2,1,0:T(8,128)(2,1)} async-done(((bf16[4,192,1024]{2,1,0:T(8,128)(2,1)}), bf16[4,192,1024]{2,1,0:T(8,128)(2,1)}, u32[]{:S(2)}, u32[]{:S(2)}) %all-to-all-start.1) | async-done | bytes 1572896 | tf_op jit(solution)/shard_map/all_to_all | solution.py:14
  76.5 4.9 %convolution_convert_fusion.1 = bf16[768,1408]{1,0:T(8,128)(2,1)S(1)} fusion(bf16[768,1024]{1,0:T(8,128)(2,1)} %bitcast.1, bf16[1408,1024]{1,0:T(8,128)(2,1)} %bitcast.85), kind=kOutput, calls=%fused_computation.3 | convolution fusion | flops 2215673856 | bytes 6619136 | tf_op jit(solution)/shard_map/dot_general | solution.py:26
  81.4 29.2 %all_to_all.62 = bf16[4,192,1408]{2,1,0:T(8,128)(2,1)S(1)} all-to-all(bf16[4,192,1408]{2,1,0:T(8,128)(2,1)S(1)} %bitcast.93), channel_id=1, replica_groups=mesh['z'=4,'x'=4,'y'=4,'c'=2] {'z'}, dimensions={0} | all-to-all | bytes 4325376 | tf_op jit(solution)/shard_map/all_to_all | solution.py:14
  112.3 4.4 %all-to-all-start.4 = ((bf16[4,192,704]{2,1,0:T(8,128)(2,1)}), bf16[4,192,704]{2,1,0:T(8,128)(2,1)}, u32[]{:S(2)}, u32[]{:S(2)}) async-start(bf16[4,192,704]{2,1,0:T(8,128)(2,1)} %broadcast_in_dim.17), calls=%async_computation.4 | async-start | bytes 2359296 | tf_op jit(solution)/shard_map/all_to_all | solution.py:14
  119.1 10.4 %all-to-all-done.4 = bf16[4,192,704]{2,1,0:T(8,128)(2,1)} async-done(((bf16[4,192,704]{2,1,0:T(8,128)(2,1)}), bf16[4,192,704]{2,1,0:T(8,128)(2,1)}, u32[]{:S(2)}, u32[]{:S(2)}) %all-to-all-start.4) | async-done | bytes 1081376 | tf_op jit(solution)/shard_map/all_to_all | solution.py:14
  137.4 18.0 %all-to-all-done.7 = bf16[4,3,352,256]{3,2,1,0:T(8,128)(2,1)S(1)} async-done(((bf16[4,3,352,256]{3,2,1,0:T(8,128)(2,1)}), bf16[4,3,352,256]{3,2,1,0:T(8,128)(2,1)S(1)}, u32[]{:S(2)}, u32[]{:S(2)}) %all-to-all-start.7) | async-done | bytes 2162720 | tf_op jit(solution)/shard_map/all_to_all | solution.py:14
  155.3 4.4 %all-to-all-start.5 = ((bf16[16,48,1024]{2,1,0:T(8,128)(2,1)}), bf16[16,48,1024]{2,1,0:T(8,128)(2,1)}, u32[]{:S(2)}, u32[]{:S(2)}) async-start(bf16[16,48,1024]{2,1,0:T(8,128)(2,1)} %bitcast.95), calls=%async_computation.5 | async-start | bytes 3145728 | tf_op jit(solution)/shard_map/all_to_all | solution.py:14
  159.8 18.8 %all_gather.3 = f32[2,1024]{1,0:T(2,128)S(1)} all-gather(f32[2,256]{1,0:T(2,128)S(1)} %pad_maximum_fusion), channel_id=1, replica_groups=mesh['z'=4,'x'=4,'y'=4,'c'=2] {'x'}, dimensions={1}, use_global_device_ids=true | all-gather | bytes 10240 | tf_op jit(solution)/shard_map/all_gather | solution.py:65
  180.3 8.3 %collective-permute-start.1 = (bf16[3,352,1024]{2,1,0:T(8,128)(2,1)}, bf16[3,352,1024]{2,1,0:T(8,128)(2,1)S(1)}, u32[]{:S(2)}, u32[]{:S(2)}) collective-permute-start(bf16[3,352,1024]{2,1,0:T(8,128)(2,1)} %bitcast.59), channel_id=1, source_target_pairs={{0,1},{1,0},{2,3},{3,2},{4,5},{5,4},{6,7},{7,6},{8,9},{9,8},{10,11... | collective-permute-start | bytes 6488072 | tf_op jit(solution)/shard_map/ppermute | solution.py:22
  191.4 6.9 %psum.21 = f32[2,48]{1,0:T(2,128)S(1)} all-reduce(f32[2,48]{1,0:T(2,128)S(1)} %pad_maximum_fusion.2), channel_id=1, replica_groups=mesh['z'=4,'x'=4,'y'=4,'c'=2] {'z'}, use_global_device_ids=true, to_apply=%region_4.5 | all-reduce | flops 96 | bytes 768 | tf_op jit(solution)/shard_map/psum | solution.py:74
  200.7 5.1 %all-to-all-start.6 = ((bf16[16,48,1024]{2,1,0:T(8,128)(2,1)}), bf16[16,48,1024]{2,1,0:T(8,128)(2,1)}, u32[]{:S(2)}, u32[]{:S(2)}) async-start(bf16[16,48,1024]{2,1,0:T(8,128)(2,1)} %broadcast_in_dim.18), calls=%async_computation.6 | async-start | bytes 3145728 | tf_op jit(solution)/shard_map/all_to_all | solution.py:14
  211.7 14.5 %all-to-all-done.6 = bf16[16,48,1024]{2,1,0:T(8,128)(2,1)} async-done(((bf16[16,48,1024]{2,1,0:T(8,128)(2,1)}), bf16[16,48,1024]{2,1,0:T(8,128)(2,1)}, u32[]{:S(2)}, u32[]{:S(2)}) %all-to-all-start.6) | async-done | bytes 1572896 | tf_op jit(solution)/shard_map/all_to_all | solution.py:14
  226.2 4.9 %convolution_convert_fusion = bf16[768,1408]{1,0:T(8,128)(2,1)S(1)} fusion(bf16[768,1024]{1,0:T(8,128)(2,1)} %bitcast.22, bf16[1408,1024]{1,0:T(8,128)(2,1)} %bitcast.86), kind=kOutput, calls=%fused_computation.2 | convolution fusion | flops 2215673856 | bytes 6619136 | tf_op jit(solution)/shard_map/dot_general | solution.py:26
  231.1 25.4 %all_to_all.63 = bf16[4,192,1408]{2,1,0:T(8,128)(2,1)S(1)} all-to-all(bf16[4,192,1408]{2,1,0:T(8,128)(2,1)S(1)} %bitcast.94), channel_id=1, replica_groups=mesh['z'=4,'x'=4,'y'=4,'c'=2] {'z'}, dimensions={0} | all-to-all | bytes 4325376 | tf_op jit(solution)/shard_map/all_to_all | solution.py:14
  257.2 13.7 %all_to_all.64 = bf16[4,192,704]{2,1,0:T(8,128)(2,1)S(1)} all-to-all(bf16[4,192,704]{2,1,0:T(8,128)(2,1)S(1)} %broadcast_in_dim.19), channel_id=1, replica_groups=mesh['z'=4,'x'=4,'y'=4,'c'=2] {'z'}, dimensions={0} | all-to-all | bytes 2162688 | tf_op jit(solution)/shard_map/all_to_all | solution.py:14
  279.2 10.2 %all-to-all-start.10 = ((bf16[16,192,256]{2,1,0:T(8,128)(2,1)}), bf16[16,192,256]{2,1,0:T(8,128)(2,1)S(1)}, u32[]{:S(2)}, u32[]{:S(2)}) async-start(bf16[16,192,256]{2,1,0:T(8,128)(2,1)} %bitcast.84), calls=%async_computation.10 | async-start | bytes 3145728 | tf_op jit(solution)/shard_map/all_to_all | solution.py:14
  289.4 19.0 %all-to-all-done.10 = bf16[16,192,256]{2,1,0:T(8,128)(2,1)S(1)} async-done(((bf16[16,192,256]{2,1,0:T(8,128)(2,1)}), bf16[16,192,256]{2,1,0:T(8,128)(2,1)S(1)}, u32[]{:S(2)}, u32[]{:S(2)}) %all-to-all-start.10) | async-done | bytes 1572896 | tf_op jit(solution)/shard_map/all_to_all | solution.py:14
  309.8 6.9 %psum.22 = f32[2,192]{1,0:T(2,128)S(1)} all-reduce(f32[2,192]{1,0:T(2,128)S(1)} %pad_maximum_fusion.1), channel_id=1, replica_groups=mesh['z'=4,'x'=4,'y'=4,'c'=2] {'z'}, use_global_device_ids=true, to_apply=%region_9.10 | all-reduce | flops 384 | bytes 3072 | tf_op jit(solution)/shard_map/psum | solution.py:84
  316.6 8.8 %psum.23 = f32[2,192]{1,0:T(2,128)S(1)} all-reduce(f32[2,192]{1,0:T(2,128)S(1)} %psum.22), channel_id=1, replica_groups=mesh['z'=4,'x'=4,'y'=4,'c'=2] {'x'}, use_global_device_ids=true, to_apply=%region_10.11 | all-reduce | flops 384 | bytes 3072 | tf_op jit(solution)/shard_map/psum | solution.py:83
  326.5 9.8 %all_to_all.65 = bf16[4,192,256]{2,1,0:T(8,128)(2,1)S(1)} all-to-all(bf16[4,192,256]{2,1,0:T(8,128)(2,1)S(1)} %broadcast_in_dim.20), channel_id=1, replica_groups=mesh['z'=4,'x'=4,'y'=4,'c'=2] {'y'}, dimensions={0} | all-to-all | bytes 786432 | tf_op jit(solution)/shard_map/all_to_all | solution.py:14
  336.4 7.4 %collective-permute-start.2 = (bf16[768,256]{1,0:T(8,128)(2,1)S(1)}, bf16[768,256]{1,0:T(8,128)(2,1)S(1)}, u32[]{:S(2)}, u32[]{:S(2)}) collective-permute-start(bf16[768,256]{1,0:T(8,128)(2,1)S(1)} %bitcast.97), channel_id=1, source_target_pairs={{0,1},{1,0},{2,3},{3,2},{4,5},{5,4},{6,7},{7,6},{8,9},{9,8},{10,11... | collective-permute-start | bytes 1179656 | tf_op jit(solution)/shard_map/ppermute | solution.py:22
  (75 shorter events, 56.2 us)
Async XLA Ops:
  0.0 40.9 %copy-start = (bf16[1536,256]{1,0:T(8,128)(2,1)S(1)}, bf16[1536,256]{1,0:T(8,128)(2,1)}, u32[]{:S(2)}) copy-start(bf16[1536,256]{1,0:T(8,128)(2,1)} %param.6) | copy-start | bytes 2359300
  38.7 18.5 %collective-permute-start = (bf16[3,352,1024]{2,1,0:T(8,128)(2,1)S(1)}, bf16[3,352,1024]{2,1,0:T(8,128)(2,1)}, u32[]{:S(2)}, u32[]{:S(2)}) collective-permute-start(bf16[3,352,1024]{2,1,0:T(8,128)(2,1)S(1)} %bitcast.81), channel_id=1, source_target_pairs={{0,1},{1,0},{2,3},{3,2},{4,5},{5,4},{6,7},{7,6},{8,9},{9,8},{10,11... | collective-permute-start | bytes 6488072 | tf_op jit(solution)/shard_map/ppermute | solution.py:22
  52.6 23.8 %all-to-all-start.1 = ((bf16[4,192,1024]{2,1,0:T(8,128)(2,1)}), bf16[4,192,1024]{2,1,0:T(8,128)(2,1)}, u32[]{:S(2)}, u32[]{:S(2)}) async-start(bf16[4,192,1024]{2,1,0:T(8,128)(2,1)} %broadcast_in_dim.16), calls=%async_computation.1 | async-start | bytes 3145728 | tf_op jit(solution)/shard_map/all_to_all | solution.py:14
  59.0 2.1 copy-start.2
  111.1 5.6 %copy-start.4 = (bf16[1,256,1408]{2,1,0:T(8,128)(2,1)S(1)}, bf16[1,256,1408]{2,1,0:T(8,128)(2,1)}, u32[]{:S(2)}) copy-start(bf16[1,256,1408]{2,1,0:T(8,128)(2,1)} %get-tuple-element.9) | copy-start | bytes 2162692
  112.3 4.7 %copy-start.5 = (bf16[1,256,1408]{2,1,0:T(8,128)(2,1)S(1)}, bf16[1,256,1408]{2,1,0:T(8,128)(2,1)}, u32[]{:S(2)}) copy-start(bf16[1,256,1408]{2,1,0:T(8,128)(2,1)} %get-tuple-element.11) | copy-start | bytes 2162692
  112.3 5.0 %copy-start.6 = (bf16[1,1408,256]{2,1,0:T(8,128)(2,1)S(1)}, bf16[1,1408,256]{2,1,0:T(8,128)(2,1)}, u32[]{:S(2)}) copy-start(bf16[1,1408,256]{2,1,0:T(8,128)(2,1)} %get-tuple-element.13) | copy-start | bytes 2162692
  112.3 17.1 %all-to-all-start.4 = ((bf16[4,192,704]{2,1,0:T(8,128)(2,1)}), bf16[4,192,704]{2,1,0:T(8,128)(2,1)}, u32[]{:S(2)}, u32[]{:S(2)}) async-start(bf16[4,192,704]{2,1,0:T(8,128)(2,1)} %broadcast_in_dim.17), calls=%async_computation.4 | async-start | bytes 2359296 | tf_op jit(solution)/shard_map/all_to_all | solution.py:14
  129.4 25.9 %all-to-all-start.7 = ((bf16[4,3,352,256]{3,2,1,0:T(8,128)(2,1)}), bf16[4,3,352,256]{3,2,1,0:T(8,128)(2,1)S(1)}, u32[]{:S(2)}, u32[]{:S(2)}) async-start(bf16[4,3,352,256]{3,2,1,0:T(8,128)(2,1)} %copy.34), calls=%async_computation.7 | async-start | bytes 4325376 | tf_op jit(solution)/shard_map/all_to_all | solution.py:14
  137.4 22.4 %copy-start.7 = (f32[2,256]{1,0:T(2,128)S(1)}, f32[2,256]{1,0:T(2,128)}, u32[]{:S(2)}) copy-start(f32[2,256]{1,0:T(2,128)} %param.10) | copy-start | bytes 6148
  137.4 22.4 %copy-start.8 = (f32[2,256]{1,0:T(2,128)S(1)}, f32[2,256]{1,0:T(2,128)}, u32[]{:S(2)}) copy-start(f32[2,256]{1,0:T(2,128)} %param.11) | copy-start | bytes 6148
  155.3 33.2 %all-to-all-start.5 = ((bf16[16,48,1024]{2,1,0:T(8,128)(2,1)}), bf16[16,48,1024]{2,1,0:T(8,128)(2,1)}, u32[]{:S(2)}, u32[]{:S(2)}) async-start(bf16[16,48,1024]{2,1,0:T(8,128)(2,1)} %bitcast.95), calls=%async_computation.5 | async-start | bytes 3145728 | tf_op jit(solution)/shard_map/all_to_all | solution.py:14
  180.3 27.3 %collective-permute-start.1 = (bf16[3,352,1024]{2,1,0:T(8,128)(2,1)}, bf16[3,352,1024]{2,1,0:T(8,128)(2,1)S(1)}, u32[]{:S(2)}, u32[]{:S(2)}) collective-permute-start(bf16[3,352,1024]{2,1,0:T(8,128)(2,1)} %bitcast.59), channel_id=1, source_target_pairs={{0,1},{1,0},{2,3},{3,2},{4,5},{5,4},{6,7},{7,6},{8,9},{9,8},{10,11... | collective-permute-start | bytes 6488072 | tf_op jit(solution)/shard_map/ppermute | solution.py:22
  200.7 25.6 %all-to-all-start.6 = ((bf16[16,48,1024]{2,1,0:T(8,128)(2,1)}), bf16[16,48,1024]{2,1,0:T(8,128)(2,1)}, u32[]{:S(2)}, u32[]{:S(2)}) async-start(bf16[16,48,1024]{2,1,0:T(8,128)(2,1)} %broadcast_in_dim.18), calls=%async_computation.6 | async-start | bytes 3145728 | tf_op jit(solution)/shard_map/all_to_all | solution.py:14
  207.7 2.0 copy-start.3
  279.2 29.2 %all-to-all-start.10 = ((bf16[16,192,256]{2,1,0:T(8,128)(2,1)}), bf16[16,192,256]{2,1,0:T(8,128)(2,1)S(1)}, u32[]{:S(2)}, u32[]{:S(2)}) async-start(bf16[16,192,256]{2,1,0:T(8,128)(2,1)} %bitcast.84), calls=%async_computation.10 | async-start | bytes 3145728 | tf_op jit(solution)/shard_map/all_to_all | solution.py:14
  308.4 37.8 %copy-start.1 = (bf16[1536,256]{1,0:T(8,128)(2,1)S(1)}, bf16[1536,256]{1,0:T(8,128)(2,1)}, u32[]{:S(2)}) copy-start(bf16[1536,256]{1,0:T(8,128)(2,1)} %param.6) | copy-start | bytes 2359300
  336.4 8.7 %collective-permute-start.2 = (bf16[768,256]{1,0:T(8,128)(2,1)S(1)}, bf16[768,256]{1,0:T(8,128)(2,1)S(1)}, u32[]{:S(2)}, u32[]{:S(2)}) collective-permute-start(bf16[768,256]{1,0:T(8,128)(2,1)S(1)} %bitcast.97), channel_id=1, source_target_pairs={{0,1},{1,0},{2,3},{3,2},{4,5},{5,4},{6,7},{7,6},{8,9},{9,8},{10,11... | collective-permute-start | bytes 1179656 | tf_op jit(solution)/shard_map/ppermute | solution.py:22
